TPU v7x, 256 devices: a whole 4x4x8 slice. The times are simulated.
256 devices in a mesh: ra: 32 (over z, y), cb: 4 (over x), dp: 2 (over core).
Axes of the slice: x: 4, y: 4, z: 8, core: 2. Of those that a mesh axis runs over, the one named last changes fastest.
Arguments:
- stream: bfloat16 [3072, 4096], P(('cb', 'dp'), 'ra'), may hold values from -20 to 20
- up_first: bfloat16 [4096, 16384], P('cb', 'ra'), may hold values from -0.09375 to 0.09375
- down_first: bfloat16 [16384, 4096], P('ra', 'cb'), may hold values from -0.046875 to 0.046875
- up_second: bfloat16 [4096, 16384], P('cb', 'ra'), may hold values from -0.09375 to 0.09375
- down_second: bfloat16 [16384, 4096], P('ra', 'cb'), may hold values from -0.046875 to 0.046875
- gain_first: float32 [4096], P('ra'), may hold values from 0.1 to 1.9
- bias_first: float32 [4096], P('ra'), may hold values from -3 to 3
- gain_second: float32 [4096], P('ra'), may hold values from 0.1 to 1.9
- bias_second: float32 [4096], P('ra'), may hold values from -3 to 3
Outputs:
- result: bfloat16 [3072, 4096], P(('cb', 'dp'), 'ra')
All inputs are finite; a program needn't handle non-finite values.
Results may differ from a plain program's by a relative error of at most 0.0093.
Values may be sent and summed in bfloat16 or wider, within the bound.
No kernel may reach another device: no remote copies, remote signals or barrier semaphores. Data moves between devices by JAX's collectives and lax.ppermute only.
A program may use at most 64 MiB of HBM per device.

v0:
```python
import jax
import jax.numpy as jnp
from jax import lax
from jax.sharding import Mesh
from jax.sharding import PartitionSpec as P

RA = ("ra_0", "ra_1")
RESID = 1.4142135
EPS = 0.5


def whole_of(shard, axes, dim):
    for axis in reversed(axes):
        shard = lax.all_gather(shard, axis, axis=dim, tiled=True)
    return shard


def cut_along(shard, dim, length):
    lengths = shard.shape
    blocks = shard.reshape(*lengths[:dim], length, lengths[dim] // length, *lengths[dim + 1 :])
    return jnp.moveaxis(blocks, dim, 0)


def summed_on_arrival(shard, axis, dim):
    length = lax.axis_size(axis)
    blocks = lax.all_to_all(cut_along(shard, dim, length), axis, 0, 0, tiled=True)
    return jnp.sum(blocks.astype(jnp.float32), axis=0)


def copy_for_each(shard, axis):
    length = lax.axis_size(axis)
    return lax.all_to_all(
        jnp.broadcast_to(shard[None], (length, *shard.shape)), axis, 0, 0, tiled=True
    )


def over_copies(shard, axis):
    everything = copy_for_each(shard, axis)
    return jnp.sum(everything, axis=0)


def in_one(arrays, axis):
    ravelled, at, done = (jnp.concatenate([a.reshape(-1) for a in arrays]), 0, [])
    subtotal = over_copies(ravelled, axis)
    for a in arrays:
        done.append(subtotal[at : at + a.size].reshape(a.shape))
        at += a.size
    return tuple(done)


def sublayer(x, up, down, gain, bias):
    whole = whole_of(x, RA, 1)
    pre = jnp.dot(
        whole, lax.all_gather(up, "cb", axis=0, tiled=True), preferred_element_type=jnp.float32
    )
    hidden = jnp.square(jax.nn.relu(pre)).astype(jnp.bfloat16)
    partial_sums = jnp.dot(
        hidden, lax.all_gather(down, "cb", axis=1, tiled=True), preferred_element_type=jnp.float32
    )
    branch = summed_on_arrival(partial_sums.astype(jnp.bfloat16), RA, 1)
    mixed = RESID * x.astype(jnp.float32) + branch
    width = mixed.shape[1] * lax.axis_size(RA)
    total, squares = in_one(
        (jnp.sum(mixed, axis=1, keepdims=True), jnp.sum(mixed * mixed, axis=1, keepdims=True)), RA
    )
    mean = total / width
    var = squares / width - mean * mean
    centered = mixed - mean
    return (centered * lax.rsqrt(var + EPS) * gain + bias).astype(jnp.bfloat16)


def body(
    stream,
    up_first,
    down_first,
    up_second,
    down_second,
    gain_first,
    bias_first,
    gain_second,
    bias_second,
):
    x = stream
    for up, down, gain, bias in (
        (up_first, down_first, gain_first, bias_first),
        (up_second, down_second, gain_second, bias_second),
    ):
        x = sublayer(x, up, down, gain, bias)
    return x


def solution(mesh):
    torus = Mesh(
        mesh.devices.reshape(8, 4, mesh.shape["cb"], mesh.shape["dp"]), ("ra_0", "ra_1", "cb", "dp")
    )
    in_specs = (
        P(("cb", "dp"), RA),
        P("cb", RA),
        P(RA, "cb"),
        P("cb", RA),
        P(RA, "cb"),
        P(RA),
        P(RA),
        P(RA),
        P(RA),
    )
    out_specs = P(("cb", "dp"), RA)
    return jax.shard_map(body, mesh=torus, in_specs=in_specs, out_specs=out_specs, check_vma=False)
```

profile of v0, /device:TPU:2, one launch (start us, length us, event | category | flops | bytes accessed | tf_op | source)
XLA Modules:
  0.0 448.1 jit_solution(4265126801284976559)
XLA Ops:
  6.5 13.8 %all_gather.24 = bf16[384,512]{1,0:T(8,128)(2,1)} all-gather(bf16[384,128]{1,0:T(8,128)(2,1)} %param.9), channel_id=1, replica_groups=mesh['ra_0'=8,'ra_1'=4,'cb'=4,'dp'=2] {'ra_1'}, dimensions={1}, use_global_device_ids=true | all-gather | bytes 491520 | tf_op jit(solution)/shard_map/all_gather | solution.py:14
  20.5 0.7 all-gather.11.cloned.1.call-update
  21.2 0.7 all-gather.9.cloned.1.call-update
  21.9 0.5 all-gather.15.cloned.1.call-update
  22.5 46.4 %all-gather.7.cloned.1.call-done = bf16[384,4096]{1,0:T(8,128)(2,1)} async-done(((bf16[384,512]{1,0:T(8,128)(2,1)}), bf16[384,4096]{1,0:T(8,128)(2,1)}) %all-gather.7.cloned.1.call-update) | async-done | bytes 3145744 | tf_op jit(solution)/shard_map/all_gather | solution.py:14
  68.9 50.6 %all-gather.11.cloned.1.call-done = bf16[512,4096]{1,0:T(8,128)(2,1)} async-done(((bf16[512,1024]{1,0:T(8,128)(2,1)}), bf16[512,4096]{1,0:T(8,128)(2,1)}) %all-gather.11.cloned.1.call-update) | async-done | bytes 4194320 | tf_op jit(solution)/shard_map/all_gather | solution.py:58
  119.4 53.0 %all-gather.9.cloned.1.call-done = bf16[4096,512]{1,0:T(8,128)(2,1)} async-done(((bf16[1024,512]{1,0:T(8,128)(2,1)}), bf16[4096,512]{1,0:T(8,128)(2,1)}) %all-gather.9.cloned.1.call-update) | async-done | bytes 4194320 | tf_op jit(solution)/shard_map/all_gather | solution.py:54
  172.4 7.8 %fusion = bf16[48,32,8,128]{3,2,1,0:T(8,128)(2,1)S(1)} fusion(bf16[512,4096]{1,0:T(8,128)(2,1)} %all-gather.11.cloned.1.call-done, bf16[384,4096]{1,0:T(8,128)(2,1)} %all-gather.7.cloned.1.call-done, bf16[4096,512]{1,0:T(8,128)(2,1)} %all-gather.9.cloned.1.call-done), kind=kOutput, calls=%fused_computation.6 | convolution fusion | flops 3223388160 | bytes 14680064 | tf_op jit(solution)/shard_map/dot_general | solution.py:57
  180.2 2.6 copy.29
  182.8 10.0 %all-to-all-start = ((bf16[32,384,128]{2,1,0:T(8,128)(2,1)}), bf16[32,384,128]{2,1,0:T(8,128)(2,1)S(1)}, u32[]{:S(2)}, u32[]{:S(2)}) async-start(bf16[32,384,128]{2,1,0:T(8,128)(2,1)} %bitcast.22), calls=%async_computation | async-start | bytes 6291456 | tf_op jit(solution)/shard_map/all_to_all | solution.py:26
  192.9 0.5 all-gather.17.cloned.1.call-update
  193.5 71.5 %all-to-all-done = bf16[32,384,128]{2,1,0:T(8,128)(2,1)S(1)} async-done(((bf16[32,384,128]{2,1,0:T(8,128)(2,1)}), bf16[32,384,128]{2,1,0:T(8,128)(2,1)S(1)}, u32[]{:S(2)}, u32[]{:S(2)}) %all-to-all-start) | async-done | bytes 3145760 | tf_op jit(solution)/shard_map/all_to_all | solution.py:26
  264.9 0.4 convert_reduce_fusion.1
  265.4 0.2 fusion.8
  265.6 16.4 %all_to_all.22 = f32[32,1,768]{2,1,0:T(1,128)S(1)} all-to-all(f32[32,1,768]{2,1,0:T(1,128)S(1)} %broadcast_in_dim.4), channel_id=1, replica_groups=mesh['ra_0'=8,'ra_1'=4,'cb'=4,'dp'=2] {'ra_0','ra_1'}, dimensions={0} | all-to-all | bytes 196608 | tf_op jit(solution)/shard_map/all_to_all | solution.py:32
  282.3 12.7 %all_gather.28 = bf16[384,512]{1,0:T(8,128)(2,1)} all-gather(bf16[384,128]{1,0:T(8,128)(2,1)S(1)} %add_convert_fusion.1), channel_id=1, replica_groups=mesh['ra_0'=8,'ra_1'=4,'cb'=4,'dp'=2] {'ra_1'}, dimensions={1}, use_global_device_ids=true | all-gather | bytes 491520 | tf_op jit(solution)/shard_map/all_gather | solution.py:14
  295.1 40.6 %all-gather.13.cloned.1.call-done = bf16[384,4096]{1,0:T(8,128)(2,1)} async-done(((bf16[384,512]{1,0:T(8,128)(2,1)}), bf16[384,4096]{1,0:T(8,128)(2,1)}) %all-gather.13.cloned.1.call-update) | async-done | bytes 3145744 | tf_op jit(solution)/shard_map/all_gather | solution.py:14
  335.7 7.8 %fusion.1 = bf16[48,32,8,128]{3,2,1,0:T(8,128)(2,1)S(1)} fusion(bf16[512,4096]{1,0:T(8,128)(2,1)} %all-gather.17.cloned.1.call-done, bf16[384,4096]{1,0:T(8,128)(2,1)} %all-gather.13.cloned.1.call-done, bf16[4096,512]{1,0:T(8,128)(2,1)} %all-gather.15.cloned.1.call-done), kind=kOutput, calls=%fused_computation.7 | convolution fusion | flops 3223388160 | bytes 14680064 | tf_op jit(solution)/shard_map/dot_general | solution.py:57
  343.5 0.9 copy.28
  344.4 79.6 %all_to_all.23 = bf16[32,384,128]{2,1,0:T(8,128)(2,1)S(1)} all-to-all(bf16[32,384,128]{2,1,0:T(8,128)(2,1)S(1)} %bitcast.23), channel_id=1, replica_groups=mesh['ra_0'=8,'ra_1'=4,'cb'=4,'dp'=2] {'ra_0','ra_1'}, dimensions={0} | all-to-all | bytes 6291456 | tf_op jit(solution)/shard_map/all_to_all | solution.py:26
  424.1 0.4 convert_reduce_fusion
  424.5 0.2 fusion.9
  424.8 15.6 %all_to_all.24 = f32[32,1,768]{2,1,0:T(1,128)S(1)} all-to-all(f32[32,1,768]{2,1,0:T(1,128)S(1)} %broadcast_in_dim.5), channel_id=1, replica_groups=mesh['ra_0'=8,'ra_1'=4,'cb'=4,'dp'=2] {'ra_0','ra_1'}, dimensions={0} | all-to-all | bytes 196608 | tf_op jit(solution)/shard_map/all_to_all | solution.py:32
  440.5 0.8 add_convert_fusion
  (29 shorter events, 0.8 us)
Async XLA Ops:
  6.5 62.3 %all-gather.7.cloned.1.call-start = ((), (), s32[]{:S(2)}) async-start(), calls=%async_computation.4 | async-start | bytes 3538944 | tf_op jit(solution)/shard_map/all_gather | solution.py:14
  20.4 99.0 %all-gather.11.cloned.1.call-start = ((), (), s32[]{:S(2)}) async-start(), calls=%async_computation.6 | async-start | bytes 5242880 | tf_op jit(solution)/shard_map/all_gather | solution.py:58
  21.2 151.2 %all-gather.9.cloned.1.call-start = ((), (), s32[]{:S(2)}) async-start(), calls=%async_computation.5 | async-start | bytes 5242880 | tf_op jit(solution)/shard_map/all_gather | solution.py:54
  21.9 273.1 %all-gather.15.cloned.1.call-start = ((), (), s32[]{:S(2)}) async-start(), calls=%async_computation.8 | async-start | bytes 5242880 | tf_op jit(solution)/shard_map/all_gather | solution.py:54
  182.8 82.5 %copy-start = (bf16[384,128]{1,0:T(8,128)(2,1)S(1)}, bf16[384,128]{1,0:T(8,128)(2,1)}, u32[]{:S(2)}) copy-start(bf16[384,128]{1,0:T(8,128)(2,1)} %param.9) | copy-start | bytes 294916
  182.8 99.3 %copy-start.1 = (f32[128]{0:T(128)S(1)}, f32[128]{0:T(128)}, u32[]{:S(2)}) copy-start(f32[128]{0:T(128)} %param.15) | copy-start | bytes 1540
  182.8 99.3 %copy-start.2 = (f32[128]{0:T(128)S(1)}, f32[128]{0:T(128)}, u32[]{:S(2)}) copy-start(f32[128]{0:T(128)} %param.14) | copy-start | bytes 1540
  182.8 82.1 %all-to-all-start = ((bf16[32,384,128]{2,1,0:T(8,128)(2,1)}), bf16[32,384,128]{2,1,0:T(8,128)(2,1)S(1)}, u32[]{:S(2)}, u32[]{:S(2)}) async-start(bf16[32,384,128]{2,1,0:T(8,128)(2,1)} %bitcast.22), calls=%async_computation | async-start | bytes 6291456 | tf_op jit(solution)/shard_map/all_to_all | solution.py:26
  192.8 102.2 %all-gather.17.cloned.1.call-start = ((), (), s32[]{:S(2)}) async-start(), calls=%async_computation.9 | async-start | bytes 5242880 | tf_op jit(solution)/shard_map/all_gather | solution.py:58
  193.4 142.3 %all-gather.13.cloned.1.call-start = ((), (), s32[]{:S(2)}) async-start(), calls=%async_computation.7 | async-start | bytes 3538944 | tf_op jit(solution)/shard_map/all_gather | solution.py:14
  344.4 96.0 %copy-start.3 = (f32[128]{0:T(128)S(1)}, f32[128]{0:T(128)}, u32[]{:S(2)}) copy-start(f32[128]{0:T(128)} %param.17) | copy-start | bytes 1540
  344.4 96.0 %copy-start.4 = (f32[128]{0:T(128)S(1)}, f32[128]{0:T(128)}, u32[]{:S(2)}) copy-start(f32[128]{0:T(128)} %param.16) | copy-start | bytes 1540
Sparse Core Ops, SparseCore 0:
  20.5 48.2 all-gather.6
  70.7 48.7 all-gather.10
  121.2 51.0 all-gather.8
  174.0 51.0 all-gather.14
  226.8 51.0 all-gather.16
  295.1 40.5 all-gather.12
where the time goes:
time: 448 us
  waiting for transfers between devices  265 us (59%)
  blocking collectives  138 us (31%)
  matrix products  15.7 us (4%)
  between operations  13.6 us (3%)
  starting transfers between devices  10.2 us (2%)
    all_gather x2, waiting for transfers between devices, whole_of(): shard = lax.all_gather(shard, axis, axis=dim, tiled=True)  87 us
    all_to_all x1, blocking collectives, summed_on_arrival(): lax.all_to_all(cut_along(shard, dim, length), axis, 0, 0, tiled=True)  79.6 us
    all_to_all x1, waiting for transfers between devices, summed_on_arrival(): lax.all_to_all(cut_along(shard, dim, length), axis, 0, 0, tiled=True)  71.5 us
    all_gather x2, waiting for transfers between devices, sublayer(): lax.all_gather(up, 'cb', axis=0, tiled=True)  53 us
    all_gather x2, waiting for transfers between devices, sublayer(): lax.all_gather(down, 'cb', axis=1, tiled=True)  50.6 us
    all_to_all x2, blocking collectives, copy_for_each(): lax.all_to_all(jnp.broadcast_to(shard[None], (length, *shard.shape)), axi...  31.9 us
    all_gather x2, blocking collectives, whole_of(): shard = lax.all_gather(shard, axis, axis=dim, tiled=True)  26.5 us
    dot_general x2, matrix products, sublayer(): jnp.dot(hidden, lax.all_gather(down, 'cb', axis=1, tiled=True), preferred...  15.7 us
  transfers between devices with their start and end apart: 7, of which 5 were waited for; matrix products, arithmetic and copies ran while one was open for 3% of the time, Pallas kernels for 0%

commit v1 on v0

--- a/solution.py
+++ b/solution.py
@@ -7,6 +7,19 @@
 RA = ("ra_0", "ra_1")
 RESID = 1.4142135
 EPS = 0.5
+
+
+def ring_gather(value, axis, dim):
+    ways = lax.axis_size(axis)
+    up = [(d, (d + 1) % ways) for d in range(ways)]
+    down = [(d, (d - 1) % ways) for d in range(ways)]
+    earlier, later = ([value], [value])
+    for _ in range(ways // 2):
+        earlier.append(lax.ppermute(earlier[-1], axis, up))
+    for _ in range((ways - 1) // 2):
+        later.append(lax.ppermute(later[-1], axis, down))
+    line = jnp.concatenate([*earlier[::-1], *later[1:]], axis=dim)
+    return jnp.roll(line, (lax.axis_index(axis) - ways // 2) * value.shape[dim], axis=dim)
 
 
 def whole_of(shard, axes, dim):
@@ -54,9 +67,7 @@
         whole, lax.all_gather(up, "cb", axis=0, tiled=True), preferred_element_type=jnp.float32
     )
     hidden = jnp.square(jax.nn.relu(pre)).astype(jnp.bfloat16)
-    partial_sums = jnp.dot(
-        hidden, lax.all_gather(down, "cb", axis=1, tiled=True), preferred_element_type=jnp.float32
-    )
+    partial_sums = jnp.dot(hidden, ring_gather(down, "cb", 1), preferred_element_type=jnp.float32)
     branch = summed_on_arrival(partial_sums.astype(jnp.bfloat16), RA, 1)
     mixed = RESID * x.astype(jnp.float32) + branch
     width = mixed.shape[1] * lax.axis_size(RA)

time: 448 us -> 406 us (0.906)
  waiting for transfers between devices: 265 us -> 205 us
  matrix products: 15.7 us -> 26.1 us
  starting transfers between devices: 10.2 us -> 17.6 us
    all_gather x2, waiting for transfers between devices: 87 us -> 1.23 us  [whole_of(): shard = lax.all_gather(shard, axis, axis=dim, tiled=True)]
    ppermute x0 -> x6, waiting for transfers between devices: none -> 80.9 us  [the longest x4 80.9 us: ring_gather(): earlier.append(lax.ppermute(earlier[-1], axis, up))]
    all_gather x2 -> x0, waiting for transfers between devices: 50.6 us -> none  [sublayer(): lax.all_gather(down, 'cb', axis=1, tiled=True)]
    dot_general x2, matrix products: 15.7 us -> 26.1 us  [sublayer(): jnp.dot(hidden, ring_gather(down, 'cb', 1), preferred_element_type=jnp.fl...]
    ppermute x0 -> x6, starting transfers between devices: none -> 7.49 us  [the longest x4 6.07 us: ring_gather(): earlier.append(lax.ppermute(earlier[-1], axis, up))]
  transfers between devices with their start and end apart: 7 -> 11, of which waited for: 5 -> 7; matrix products, arithmetic and copies ran while one was open for 3% -> 0% of each run, Pallas kernels for 0% -> 0%
where the time goes in v1:
time: 406 us; the launch traced here: 405 us
  waiting for transfers between devices  205 us (50%)
  blocking collectives  136 us (33%)
  matrix products  26.1 us (6%)
  starting transfers between devices  17.6 us (4%)
  between operations  13.3 us (3%)
  local copies, waits for them, and re-layouts  4.6 us (1%)
    ppermute x4, waiting for transfers between devices, ring_gather(): earlier.append(lax.ppermute(earlier[-1], axis, up))  80.9 us
    all_to_all x1, blocking collectives, summed_on_arrival(): lax.all_to_all(cut_along(shard, dim, length), axis, 0, 0, tiled=True)  77.2 us
    all_to_all x1, waiting for transfers between devices, summed_on_arrival(): lax.all_to_all(cut_along(shard, dim, length), axis, 0, 0, tiled=True)  71.3 us
    all_gather x2, waiting for transfers between devices, sublayer(): lax.all_gather(up, 'cb', axis=0, tiled=True)  50.6 us
    all_to_all x2, blocking collectives, copy_for_each(): lax.all_to_all(jnp.broadcast_to(shard[None], (length, *shard.shape)), axi...  32.1 us
    all_gather x2, blocking collectives, whole_of(): shard = lax.all_gather(shard, axis, axis=dim, tiled=True)  26.5 us
    dot_general x2, matrix products, sublayer(): jnp.dot(hidden, ring_gather(down, 'cb', 1), preferred_element_type=jnp.fl...  26.1 us
    all_to_all x1, starting transfers between devices, summed_on_arrival(): lax.all_to_all(cut_along(shard, dim, length), axis, 0, 0, tiled=True)  9.98 us
  transfers between devices with their start and end apart: 11, of which 7 were waited for; matrix products, arithmetic and copies ran while one was open for 0% of the time, Pallas kernels for 0%

profile of v1, /device:TPU:2, one launch (start us, length us, event | category | flops | bytes accessed | tf_op | source)
XLA Modules:
  0.0 405.4 jit_solution(14268393200346028312)
XLA Ops:
  6.5 13.8 %all_gather.18 = bf16[384,512]{1,0:T(8,128)(2,1)} all-gather(bf16[384,128]{1,0:T(8,128)(2,1)} %param.11), channel_id=1, replica_groups=mesh['ra_0'=8,'ra_1'=4,'cb'=4,'dp'=2] {'ra_1'}, dimensions={1}, use_global_device_ids=true | all-gather | bytes 491520 | tf_op jit(solution)/shard_map/all_gather | solution.py:27
  21.2 1.6 collective-permute-start
  23.3 21.6 %collective-permute-done = bf16[512,1024]{1,0:T(8,128)(2,1)S(1)} collective-permute-done((bf16[512,1024]{1,0:T(8,128)(2,1)}, bf16[512,1024]{1,0:T(8,128)(2,1)S(1)}, u32[]{:S(2)}, u32[]{:S(2)}) %collective-permute-start) | collective-permute-done | bytes 1048608 | tf_op jit(solution)/shard_map/ppermute | solution.py:18
  44.9 1.5 collective-permute-start.1
  46.4 21.2 %collective-permute-done.1 = bf16[512,1024]{1,0:T(8,128)(2,1)S(1)} collective-permute-done((bf16[512,1024]{1,0:T(8,128)(2,1)S(1)}, bf16[512,1024]{1,0:T(8,128)(2,1)S(1)}, u32[]{:S(2)}, u32[]{:S(2)}) %collective-permute-start.1) | collective-permute-done | bytes 1048608 | tf_op jit(solution)/shard_map/ppermute | solution.py:18
  67.6 1.2 all-gather.5.cloned.1.call-done
  68.8 50.6 %all-gather.7.cloned.1.call-done = bf16[4096,512]{1,0:T(8,128)(2,1)} async-done(((bf16[1024,512]{1,0:T(8,128)(2,1)}), bf16[4096,512]{1,0:T(8,128)(2,1)}) %all-gather.7.cloned.1.call-update) | async-done | bytes 4194320 | tf_op jit(solution)/shard_map/all_gather | solution.py:67
  119.4 13.1 %fusion.18 = bf16[48,32,8,128]{3,2,1,0:T(8,128)(2,1)S(1)} fusion(s32[]{:T(128)S(6)} %select_n.13, bf16[512,1024]{1,0:T(8,128)(2,1)} %copy-done.7, bf16[512,1024]{1,0:T(8,128)(2,1)} %copy-done.5, bf16[512,1024]{1,0:T(8,128)(2,1)} %param.13, bf16[512,1024]{1,0:T(8,128)(2,1)} %copy-done.6, bf16[384,4096]{1,0:T(8,128)(2,1)} %all-gather.5.cloned.1.call-done, ...), kind=kOutput, calls=%fused_computation.36 | convolution fusion | flops 3256942592 | bytes 14680068 | tf_op jit(solution)/shard_map/dot_general | solution.py:70
  132.5 2.5 copy.29
  135.0 10.0 %all-to-all-start = ((bf16[32,384,128]{2,1,0:T(8,128)(2,1)}), bf16[32,384,128]{2,1,0:T(8,128)(2,1)S(1)}, u32[]{:S(2)}, u32[]{:S(2)}) async-start(bf16[32,384,128]{2,1,0:T(8,128)(2,1)} %bitcast.20), calls=%async_computation | async-start | bytes 6291456 | tf_op jit(solution)/shard_map/all_to_all | solution.py:39
  145.8 71.3 %all-to-all-done = bf16[32,384,128]{2,1,0:T(8,128)(2,1)S(1)} async-done(((bf16[32,384,128]{2,1,0:T(8,128)(2,1)}), bf16[32,384,128]{2,1,0:T(8,128)(2,1)S(1)}, u32[]{:S(2)}, u32[]{:S(2)}) %all-to-all-start) | async-done | bytes 3145760 | tf_op jit(solution)/shard_map/all_to_all | solution.py:39
  217.8 16.4 %all_to_all.22 = f32[32,1,768]{2,1,0:T(1,128)S(1)} all-to-all(f32[32,1,768]{2,1,0:T(1,128)S(1)} %broadcast_in_dim.4), channel_id=1, replica_groups=mesh['ra_0'=8,'ra_1'=4,'cb'=4,'dp'=2] {'ra_0','ra_1'}, dimensions={0} | all-to-all | bytes 196608 | tf_op jit(solution)/shard_map/all_to_all | solution.py:45
  234.5 12.7 %all_gather.21 = bf16[384,512]{1,0:T(8,128)(2,1)} all-gather(bf16[384,128]{1,0:T(8,128)(2,1)S(1)} %add_convert_fusion.1), channel_id=1, replica_groups=mesh['ra_0'=8,'ra_1'=4,'cb'=4,'dp'=2] {'ra_1'}, dimensions={1}, use_global_device_ids=true | all-gather | bytes 491520 | tf_op jit(solution)/shard_map/all_gather | solution.py:27
  247.2 1.2 collective-permute-start.3
  248.4 0.9 collective-permute-start.5
  249.3 19.7 %collective-permute-done.3 = bf16[512,1024]{1,0:T(8,128)(2,1)S(1)} collective-permute-done((bf16[512,1024]{1,0:T(8,128)(2,1)}, bf16[512,1024]{1,0:T(8,128)(2,1)S(1)}, u32[]{:S(2)}, u32[]{:S(2)}) %collective-permute-start.3) | collective-permute-done | bytes 1048608 | tf_op jit(solution)/shard_map/ppermute | solution.py:18
  269.0 1.1 copy-done.8
  270.1 1.8 collective-permute-start.4
  271.9 18.4 %collective-permute-done.4 = bf16[512,1024]{1,0:T(8,128)(2,1)} collective-permute-done((bf16[512,1024]{1,0:T(8,128)(2,1)S(1)}, bf16[512,1024]{1,0:T(8,128)(2,1)}, u32[]{:S(2)}, u32[]{:S(2)}) %collective-permute-start.4) | collective-permute-done | bytes 1048608 | tf_op jit(solution)/shard_map/ppermute | solution.py:18
  290.3 13.1 %fusion.21 = bf16[48,32,8,128]{3,2,1,0:T(8,128)(2,1)S(1)} fusion(s32[]{:T(128)S(6)} %select_n.13, bf16[512,1024]{1,0:T(8,128)(2,1)} %collective-permute-done.4, bf16[512,1024]{1,0:T(8,128)(2,1)} %copy-done.8, bf16[512,1024]{1,0:T(8,128)(2,1)} %param.15, bf16[512,1024]{1,0:T(8,128)(2,1)} %collective-permute-done.5, ...), kind=kOutput, calls=%fused_computation.37 | convolution fusion | flops 3256942592 | bytes 14680068 | tf_op jit(solution)/shard_map/dot_general | solution.py:70
  303.4 0.9 copy.28
  304.2 77.2 %all_to_all.23 = bf16[32,384,128]{2,1,0:T(8,128)(2,1)S(1)} all-to-all(bf16[32,384,128]{2,1,0:T(8,128)(2,1)S(1)} %bitcast.21), channel_id=1, replica_groups=mesh['ra_0'=8,'ra_1'=4,'cb'=4,'dp'=2] {'ra_0','ra_1'}, dimensions={0} | all-to-all | bytes 6291456 | tf_op jit(solution)/shard_map/all_to_all | solution.py:39
  382.2 15.7 %all_to_all.24 = f32[32,1,768]{2,1,0:T(1,128)S(1)} all-to-all(f32[32,1,768]{2,1,0:T(1,128)S(1)} %broadcast_in_dim.5), channel_id=1, replica_groups=mesh['ra_0'=8,'ra_1'=4,'cb'=4,'dp'=2] {'ra_0','ra_1'}, dimensions={0} | all-to-all | bytes 196608 | tf_op jit(solution)/shard_map/all_to_all | solution.py:45
  398.0 0.8 add_convert_fusion
  (43 shorter events, 3.8 us)
Async XLA Ops:
  6.5 62.3 %all-gather.5.cloned.1.call-start = ((), (), s32[]{:S(2)}) async-start(), calls=%async_computation.4 | async-start | bytes 3538944 | tf_op jit(solution)/shard_map/all_gather | solution.py:27
  20.4 99.0 %all-gather.7.cloned.1.call-start = ((), (), s32[]{:S(2)}) async-start(), calls=%async_computation.5 | async-start | bytes 5242880 | tf_op jit(solution)/shard_map/all_gather | solution.py:67
  21.2 23.7 %collective-permute-start = (bf16[512,1024]{1,0:T(8,128)(2,1)}, bf16[512,1024]{1,0:T(8,128)(2,1)S(1)}, u32[]{:S(2)}, u32[]{:S(2)}) collective-permute-start(bf16[512,1024]{1,0:T(8,128)(2,1)} %param.13), channel_id=1, source_target_pairs={{0,2},{2,4},{4,6},{6,0},{1,3},{3,5},{5,7},{7,1},{8,10},{10,12},{12... | collective-permute-start | bytes 3145736 | tf_op jit(solution)/shard_map/ppermute | solution.py:18
  22.7 23.7 %collective-permute-start.2 = (bf16[512,1024]{1,0:T(8,128)(2,1)}, bf16[512,1024]{1,0:T(8,128)(2,1)S(1)}, u32[]{:S(2)}, u32[]{:S(2)}) collective-permute-start(bf16[512,1024]{1,0:T(8,128)(2,1)} %param.13), channel_id=1, source_target_pairs={{0,6},{2,0},{4,2},{6,4},{1,7},{3,1},{5,3},{7,5},{8,14},{10,8},{12,... | collective-permute-start | bytes 3145736 | tf_op jit(solution)/shard_map/ppermute | solution.py:20
  44.9 23.9 %copy-start.5 = (bf16[512,1024]{1,0:T(8,128)(2,1)}, bf16[512,1024]{1,0:T(8,128)(2,1)S(1)}, u32[]{:S(2)}) copy-start(bf16[512,1024]{1,0:T(8,128)(2,1)S(1)} %collective-permute-done) | copy-start | bytes 3145732
  44.9 22.7 %collective-permute-start.1 = (bf16[512,1024]{1,0:T(8,128)(2,1)S(1)}, bf16[512,1024]{1,0:T(8,128)(2,1)S(1)}, u32[]{:S(2)}, u32[]{:S(2)}) collective-permute-start(bf16[512,1024]{1,0:T(8,128)(2,1)S(1)} %collective-permute-done), channel_id=1, source_target_pairs={{0,2},{2,4},{4,6},{6,0},{1,3},{3,5},{5,7},{7,1},{8,10},{10,12},{12... | collective-permute-start | bytes 3145736 | tf_op jit(solution)/shard_map/ppermute | solution.py:18
  46.4 22.4 %copy-start.6 = (bf16[512,1024]{1,0:T(8,128)(2,1)}, bf16[512,1024]{1,0:T(8,128)(2,1)S(1)}, u32[]{:S(2)}) copy-start(bf16[512,1024]{1,0:T(8,128)(2,1)S(1)} %collective-permute-done.2) | copy-start | bytes 3145732
  67.6 1.2 copy-start.7
  135.0 82.5 %copy-start = (bf16[384,128]{1,0:T(8,128)(2,1)S(1)}, bf16[384,128]{1,0:T(8,128)(2,1)}, u32[]{:S(2)}) copy-start(bf16[384,128]{1,0:T(8,128)(2,1)} %param.11) | copy-start | bytes 294916
  135.0 99.3 %copy-start.1 = (f32[128]{0:T(128)S(1)}, f32[128]{0:T(128)}, u32[]{:S(2)}) copy-start(f32[128]{0:T(128)} %param.17) | copy-start | bytes 1540
  135.0 99.3 %copy-start.2 = (f32[128]{0:T(128)S(1)}, f32[128]{0:T(128)}, u32[]{:S(2)}) copy-start(f32[128]{0:T(128)} %param.16) | copy-start | bytes 1540
  135.0 82.1 %all-to-all-start = ((bf16[32,384,128]{2,1,0:T(8,128)(2,1)}), bf16[32,384,128]{2,1,0:T(8,128)(2,1)S(1)}, u32[]{:S(2)}, u32[]{:S(2)}) async-start(bf16[32,384,128]{2,1,0:T(8,128)(2,1)} %bitcast.20), calls=%async_computation | async-start | bytes 6291456 | tf_op jit(solution)/shard_map/all_to_all | solution.py:39
  145.0 145.3 %all-gather.11.cloned.1.call-start = ((), (), s32[]{:S(2)}) async-start(), calls=%async_computation.7 | async-start | bytes 5242880 | tf_op jit(solution)/shard_map/all_gather | solution.py:67
  145.7 144.5 %all-gather.9.cloned.1.call-start = ((), (), s32[]{:S(2)}) async-start(), calls=%async_computation.6 | async-start | bytes 3538944 | tf_op jit(solution)/shard_map/all_gather | solution.py:27
  247.2 21.8 %collective-permute-start.3 = (bf16[512,1024]{1,0:T(8,128)(2,1)}, bf16[512,1024]{1,0:T(8,128)(2,1)S(1)}, u32[]{:S(2)}, u32[]{:S(2)}) collective-permute-start(bf16[512,1024]{1,0:T(8,128)(2,1)} %param.15), channel_id=1, source_target_pairs={{0,2},{2,4},{4,6},{6,0},{1,3},{3,5},{5,7},{7,1},{8,10},{10,12},{12... | collective-permute-start | bytes 3145736 | tf_op jit(solution)/shard_map/ppermute | solution.py:18
  248.4 23.4 %collective-permute-start.5 = (bf16[512,1024]{1,0:T(8,128)(2,1)}, bf16[512,1024]{1,0:T(8,128)(2,1)}, u32[]{:S(2)}, u32[]{:S(2)}) collective-permute-start(bf16[512,1024]{1,0:T(8,128)(2,1)} %param.15), channel_id=1, source_target_pairs={{0,6},{2,0},{4,2},{6,4},{1,7},{3,1},{5,3},{7,5},{8,14},{10,8},{12,... | collective-permute-start | bytes 3145736 | tf_op jit(solution)/shard_map/ppermute | solution.py:20
  269.0 1.1 copy-start.8
  270.1 20.2 %collective-permute-start.4 = (bf16[512,1024]{1,0:T(8,128)(2,1)S(1)}, bf16[512,1024]{1,0:T(8,128)(2,1)}, u32[]{:S(2)}, u32[]{:S(2)}) collective-permute-start(bf16[512,1024]{1,0:T(8,128)(2,1)S(1)} %collective-permute-done.3), channel_id=1, source_target_pairs={{0,2},{2,4},{4,6},{6,0},{1,3},{3,5},{5,7},{7,1},{8,10},{10,12},{12... | collective-permute-start | bytes 3145736 | tf_op jit(solution)/shard_map/ppermute | solution.py:18
  304.2 93.8 %copy-start.3 = (f32[128]{0:T(128)S(1)}, f32[128]{0:T(128)}, u32[]{:S(2)}) copy-start(f32[128]{0:T(128)} %param.19) | copy-start | bytes 1540
  304.2 93.8 %copy-start.4 = (f32[128]{0:T(128)S(1)}, f32[128]{0:T(128)}, u32[]{:S(2)}) copy-start(f32[128]{0:T(128)} %param.18) | copy-start | bytes 1540
Sparse Core Ops, SparseCore 0:
  20.5 48.2 all-gather.4
  70.6 48.7 all-gather.6
  147.6 51.0 all-gather.10
  247.3 40.4 all-gather.8
